TPU v7x, 512 devices: a whole 4x8x8 slice. The times are simulated.
512 devices in a mesh: ep: 32 (over z, x), tp: 16 (over y, core).
Axes of the slice: x: 4, y: 8, z: 8, core: 2. Of those that a mesh axis runs over, the one named last changes fastest.
Arguments:
- queries: bfloat16 [16384, 1024], P('ep', 'tp'), may hold values from -6 to 6
- key_input: bfloat16 [16384, 256], P('ep'), may hold values from -6 to 6
- value_input: bfloat16 [16384, 256], P('ep'), may hold values from -6 to 6
- query_gain: float32 [64], replicated, may hold values from 0.1 to 1.9
- key_gain: float32 [64], replicated, may hold values from 0.1 to 1.9
- mix_out_weight: bfloat16 [1024, 2048], P('tp'), may hold values from -0.1875 to 0.1875
- expert_input: bfloat16 [5120, 2048], P('ep'), may hold values from -6 to 6
- ffn_gain: float32 [2048], replicated, may hold values from 0.1 to 1.9
- routes: int32 [5120, 2], P('ep'), may hold values from 0 to 31, all different within a row; in each aligned block of 160 rows (0 to 159, 160 to 319, ...) at most 15 rows name the same one
- route_scores: float32 [5120, 2], P('ep'), may hold values from 0.1 to 1
- gate_weight: bfloat16 [32, 2048, 4096], P('ep', None, 'tp'), may hold values from -0.125 to 0.125
- up_weight: bfloat16 [32, 2048, 4096], P('ep', None, 'tp'), may hold values from -0.125 to 0.125
- down_weight: bfloat16 [32, 4096, 2048], P('ep', 'tp'), may hold values from -0.09375 to 0.09375
Outputs:
- mixed_rows: bfloat16 [16384, 2048], P(('ep', 'tp'))
- expert_out: bfloat16 [5120, 2048], P('ep', 'tp')
Inputs may be any that keep to these rules, and one draw needn't show every extreme that they name: `routes`: each row names 2 different experts. Within the rows of one index of ep (aligned blocks of 160 rows) no expert is named by more than 15 rows, and in every draw some expert is named by exactly 15 rows of some block.
All inputs are finite; a program needn't handle non-finite values.
Results may differ from a plain program's by a relative error of at most 0.019.
The roundings to bfloat16 on the way count: a program that leaves them out, or rounds other values in their place, can miss the bound.
Values may be sent and summed in bfloat16 or wider, within the bound.
A program may use at most 64 MiB of HBM per device.

v0:
```python
import contextlib
import functools
import math
from types import SimpleNamespace

import jax
import jax.numpy as jnp
import numpy as np
from jax import lax
from jax.experimental import pallas as pl
from jax.experimental.pallas import tpu as pltpu
from jax.sharding import PartitionSpec as P

HD = 64
GRID_W = 64
EPSILON = 1e-06
ROPE_BASE = 10000.0
SLOTS = 16
CHUNKS = 4
MESH = pl.DeviceIdType.MESH
F32 = jnp.float32
BF16 = jnp.bfloat16
TRACE = False


def scope(name):
    return jax.named_scope(name) if TRACE else contextlib.nullcontext()


def angle_tables(rows):
    quarter = HD // 4
    inverse = (ROPE_BASE ** (-np.arange(quarter, dtype=np.float32) / quarter)).astype(np.float32)
    lane = np.arange(2 * HD)
    freq = inverse[lane % quarter]
    is_row = (lane % HD) < HD // 2
    sign = np.where((lane // quarter) % 2 == 0, -1.0, 1.0).astype(np.float32)

    def table(count, keep):
        angle = (np.arange(count, dtype=np.float32)[:, None] * freq[None, :]).astype(np.float32)
        cos = np.where(keep, np.cos(angle), 0.0).astype(np.float32)
        sin = np.where(keep, np.sin(angle) * sign, 0.0).astype(np.float32)
        return cos, sin

    return table(rows, is_row) + table(GRID_W, ~is_row)


def kernel(
    g,
    queries_h,
    keys_h,
    values_h,
    key_gain_h,
    query_gain_h,
    row_cos_h,
    row_sin_h,
    col_cos_h,
    col_sin_h,
    tokens,
    routes_h,
    scores_h,
    ffn_gain_h,
    mix_w,
    gate_w,
    up_w,
    down_w,
    mixed_out,
    expert_out,
    kv,
    q_own,
    q_all,
    o_acc,
    o_out,
    o_in,
    att_out,
    att_in,
    att_row,
    w_all,
    tok_own,
    outbound,
    slots,
    wg,
    wu,
    wd,
    gate_acc,
    up_acc,
    sq_acc,
    hidden,
    ring_out,
    ring_in,
    rows_out,
    rows_in,
    hot,
    share,
    ring_part,
    q_raw,
    k_raw,
    v_raw,
    key_gain,
    query_gain,
    row_cos,
    row_sin,
    col_cos,
    col_sin,
    routes,
    scores,
    ffn_gain,
    sem_local,
    sem_kv_s,
    sem_kv_r,
    sem_kvf_s,
    sem_kvf_r,
    sem_q_s,
    sem_q_r,
    sem_o_s,
    sem_o_r,
    sem_a_s,
    sem_a_r,
    sem_w_s,
    sem_w_r,
    sem_wf_s,
    sem_wf_r,
    sem_wx_s,
    sem_wx_r,
    sem_ex_s,
    sem_ex_r,
    sem_d_s,
    sem_d_r,
    sem_b_s,
    sem_b_r,
    sem_c_s,
    sem_c_r,
    sem_r_s,
    sem_r_r,
):
    nz, nx, ny, ep, tp = g.nz, g.nx, g.ny, g.nz * g.nx, g.ny * 2
    half_ep = ep // 2
    me_e, me_t = lax.axis_index("ep"), lax.axis_index("tp")
    z, x = me_e // nx, me_e % nx
    y, c = me_t // 2, me_t % 2
    sib = me_t + 1 - 2 * c
    own_half = me_e // half_ep
    tq, tok, d, ff = g.tq, g.tok, g.d, g.ff
    feat = d // 4
    par = y % 2

    def send(src, dst, ssem, rsem, to_e, to_t):
        return pltpu.make_async_remote_copy(
            src_ref=src, dst_ref=dst, send_sem=ssem, recv_sem=rsem,
            device_id=(to_e, to_t), device_id_type=MESH,
        )

    def arrived(dst, rsem):
        send(dst, dst, rsem, rsem, me_e, sib).wait_recv()

    def left(src, ssem):
        send(src, src, ssem, ssem, me_e, sib).wait_send()

    def al(v, m):
        return pl.multiple_of(v, m)

    barrier = pltpu.get_barrier_semaphore()

    def greet_plane(i, _):
        pl.semaphore_signal(barrier, inc=1, device_id=((me_e + i) % ep, me_t), device_id_type=MESH)
        pl.semaphore_signal(barrier, inc=1, device_id=((me_e + i) % ep, sib), device_id_type=MESH)
        return 0

    def greet_line(i, _):
        pl.semaphore_signal(barrier, inc=1, device_id=(me_e, (me_t + i) % tp), device_id_type=MESH)
        return 0

    lax.fori_loop(1, ep, greet_plane, 0)
    lax.fori_loop(1, tp, greet_line, 0)

    feat_at = al((par * 2 + c) * feat, feat)
    dh = d // 2
    col_half = x % 2
    cols_mine = pl.ds(al(col_half * dh, dh), dh)
    cols_other = pl.ds(al((1 - col_half) * dh, dh), dh)
    blocks = tq // GRID_W
    head = me_t * g.kv_heads // tp
    head_at = al((head // 2) * 2 * HD, 2 * HD) if g.kv_heads > 1 else 0
    head_lanes = pl.ds(head_at, 2 * HD) if g.kv_heads > 1 else pl.ds(0, HD)
    kv_lanes = slice(0, 2 * HD) if g.kv_heads > 1 else slice(0, HD)
    pairs = [
        (routes_h, routes),
        (scores_h, scores),
        (tokens.at[:, pl.ds(feat_at, feat)], tok_own),
        (queries_h, q_raw),
        (keys_h.at[:, head_lanes], k_raw.at[:, kv_lanes]),
        (values_h.at[:, head_lanes], v_raw.at[:, kv_lanes]),
        (key_gain_h, key_gain),
        (query_gain_h, query_gain),
        (row_cos_h.at[pl.ds(me_e * blocks, blocks)], row_cos),
        (row_sin_h.at[pl.ds(me_e * blocks, blocks)], row_sin),
        (col_cos_h, col_cos),
        (col_sin_h, col_sin),
        (mix_w.at[:, cols_mine], w_all.at[y, c, :, cols_mine]),
        (gate_w.at[0], wg.at[c]),
        (up_w.at[0], wu.at[c]),
        (down_w.at[0], wd.at[pl.ds(al(c * ff, ff), ff)]),
        (ffn_gain_h, ffn_gain),
    ]
    loads = [pltpu.make_async_copy(a, b, sem_local.at[i]) for i, (a, b) in enumerate(pairs)]
    for copy in loads:
        copy.start()

    for copy in loads[0:2]:
        copy.wait()
    r0, r1 = routes[0:1, :], routes[1:2, :]
    rows_e = lax.broadcasted_iota(jnp.int32, (ep, tok), 0)
    hit0 = (rows_e == r0).astype(F32)
    hit1 = (rows_e == r1).astype(F32)
    before = (
        lax.broadcasted_iota(jnp.int32, (tok, tok), 0) < lax.broadcasted_iota(jnp.int32, (tok, tok), 1)
    ).astype(BF16)
    count = jnp.dot((hit0 + hit1).astype(BF16), before, preferred_element_type=F32)
    slot0 = r0 * SLOTS + jnp.sum(count * hit0, axis=0, keepdims=True).astype(jnp.int32)
    slot1 = r1 * SLOTS + jnp.sum(count * hit1, axis=0, keepdims=True).astype(jnp.int32)
    rows_s = lax.broadcasted_iota(jnp.int32, (ep * SLOTS, tok), 0)
    to_slots = ((rows_s == slot0) | (rows_s == slot1)).astype(BF16)
    loads[2].wait()
    outbound[...] = jnp.dot(to_slots, tok_own[...], preferred_element_type=F32).astype(BF16)

    lane = lax.broadcasted_iota(jnp.int32, (GRID_W, 2 * HD), 1)
    low = lane < HD
    is_u = (lane // (HD // 4)) % 2 == 0
    for copy in loads[3:12]:
        copy.wait()
    gain = jnp.concatenate([key_gain[...], query_gain[...]], axis=1)
    odd = head % 2 == 1
    q_wide = jnp.transpose(jnp.concatenate([q_raw[...], q_raw[...]], axis=0).astype(F32))
    if g.kv_heads > 1:
        k_all, v_all = k_raw[...].astype(F32), v_raw[...].astype(F32)
        k_wide = jnp.where(odd, pltpu.roll(k_all, HD, 1), k_all)
        v_wide = jnp.where(odd, v_all, pltpu.roll(v_all, HD, 1))
    else:
        k_wide = jnp.concatenate([k_raw[:, 0:HD]] * 2, axis=1).astype(F32)
        v_wide = jnp.concatenate([v_raw[:, 0:HD]] * 2, axis=1).astype(F32)
    for b in range(blocks):
        at = b * GRID_W
        v = jnp.where(low, k_wide[at : at + GRID_W], q_wide[at : at + GRID_W])
        sq = v * v
        s_low = jnp.sum(jnp.where(low, sq, 0.0), axis=1, keepdims=True)
        s_high = jnp.sum(jnp.where(low, 0.0, sq), axis=1, keepdims=True)
        scale = jnp.where(low, lax.rsqrt(s_low * (1.0 / HD) + EPSILON), lax.rsqrt(s_high * (1.0 / HD) + EPSILON))
        n = v * scale * gain
        cos = col_cos[...] + row_cos[b : b + 1, :]
        sin = col_sin[...] + row_sin[b : b + 1, :]
        swapped = jnp.where(is_u, pltpu.roll(n, 2 * HD - HD // 4, 1), pltpu.roll(n, HD // 4, 1))
        turned = n * cos + swapped * sin
        kv[z, at : at + GRID_W, :] = jnp.where(low, turned, v_wide[at : at + GRID_W]).astype(BF16)
        att_row[at : at + GRID_W, :] = turned
    q_own[...] = jnp.transpose(att_row[...])[HD : 2 * HD, :].astype(BF16)

    with scope("barrier"):
        pl.semaphore_wait(barrier, 2 * (ep - 1) + tp - 1)

    slot_at = al((me_e % half_ep) * SLOTS, SLOTS)
    to_core = y * 2 + own_half

    fw = feat // 2

    def wave_lanes(wave):
        return pl.ds(wave * fw, fw), pl.ds(al(feat_at + wave * fw, fw), fw)

    def dispatch(i, wave):
        to_e = (me_e + i) % ep
        return send(
            outbound.at[pl.ds(al(to_e * SLOTS, SLOTS), SLOTS), wave_lanes(wave)[0]],
            slots.at[pl.ds(slot_at, SLOTS), wave_lanes(wave)[1]],
            sem_d_s.at[wave, i], sem_d_r.at[wave, (me_e % half_ep) * 2 + c], to_e, to_core,
        )

    def dispatch_self(wave):
        return pltpu.make_async_copy(
            outbound.at[pl.ds(al(me_e * SLOTS, SLOTS), SLOTS), wave_lanes(wave)[0]],
            slots.at[pl.ds(slot_at, SLOTS), wave_lanes(wave)[1]],
            sem_d_r.at[wave, (me_e % half_ep) * 2 + c],
        )

    def q_copy(i):
        return send(q_own, q_all.at[x], sem_q_s.at[i], sem_q_r.at[x], z * nx + (x + i) % nx, me_t)

    q_all[x] = q_own[...]
    for i in range(1, nx):
        q_copy(i).start()

    hq = tq // 2
    kv_mine = pl.ds(al(c * hq, hq), hq)
    kv_other = pl.ds(al((1 - c) * hq, hq), hq)

    half_z = nz // 2
    way_c = 1 - 2 * c
    chain = [(way, m) for m in range(1, half_z + 1) for way in (1, -1) if way == 1 or m < half_z]

    def shard(way, m):
        return (z + nz - way * way_c * m) % nz

    def kv_pass(way, m):
        b = kv.at[shard(way, m), kv_mine]
        to_z = (z + nz + way * way_c) % nz
        at = 0 if way == 1 else 1
        return send(b, b, sem_kv_s.at[at, m], sem_kv_r.at[shard(way, m)], to_z * nx + x, me_t)

    def kv_passes(way, m):
        return m < half_z if way == 1 else m < half_z - 1

    for way in (1, -1):
        if kv_passes(way, 0):
            kv_pass(way, 0).start()

    near = ep // 4
    for wave in range(2):

        def dispatch_start(i, _):
            dispatch(i, wave).start()
            return 0

        lax.fori_loop(near, ep - near, dispatch_start, 0)
        lax.fori_loop(1, near, dispatch_start, 0)
        lax.fori_loop(ep - near, ep, dispatch_start, 0)

        @pl.when(c == own_half)
        def _():
            dispatch_self(wave).start()

        @pl.when(c != own_half)
        def _():
            dispatch(0, wave).start()

    for copy in loads[12:]:
        copy.wait()

    extra = [
        send(wg.at[c], wg.at[c], sem_ex_s.at[0], sem_ex_r.at[0], me_e, sib),
        send(wu.at[c], wu.at[c], sem_ex_s.at[1], sem_ex_r.at[1], me_e, sib),
        send(
            wd.at[pl.ds(al(c * ff, ff), ff)], wd.at[pl.ds(al(c * ff, ff), ff)],
            sem_ex_s.at[2], sem_ex_r.at[2], me_e, sib,
        ),
    ]

    def extra_start():
        for copy in extra:
            copy.start()

    half_y = ny // 2
    right = ((y + 1) % ny) * 2 + c
    leftward = ((y + ny - 1) % ny) * 2 + c
    ahead = ((y + ny + way_c) % ny) * 2 + c
    behind = ((y + ny - way_c) % ny) * 2 + c

    def w_block(s):
        return w_all.at[(y + ny + ny - way_c * s) % ny, c, :, cols_mine]

    def w_ahead(s):
        return send(w_block(s), w_block(s), sem_w_s.at[0, s], sem_w_r.at[0, s], me_e, ahead)

    def w_behind(s):
        return send(w_block(-s), w_block(-s), sem_w_s.at[1, s], sem_w_r.at[1, s], me_e, behind)

    def w_fresh(s):
        return [s] if s in (0, half_y) else [s, -s]

    def w_row(r):
        return (y + ny + ny - way_c * r) % ny

    def w_quarter(r, k, other):
        half = 1 - col_half if other else col_half
        return w_all.at[w_row(r), c, :, pl.ds(al(half * dh + k * (dh // 2), dh // 2), dh // 2)]

    def w_swap(r, k):
        to_x = (x + nx - 1) % nx if k == 0 else (x + 1) % nx
        q = w_quarter(r, k, False)
        return send(q, q, sem_wx_s.at[k, w_row(r)], sem_wx_r.at[k, w_row(r)], z * nx + to_x, me_t)

    def w_twin(r):
        b = w_block(r)
        return send(b, b, sem_wf_s.at[w_row(r)], sem_wf_r.at[w_row(r)], me_e, sib)

    def w_step(s):
        if s > 0:
            arrived(w_block(s), sem_w_r.at[0, s - 1])
            if s < half_y:
                arrived(w_block(-s), sem_w_r.at[1, s - 1])
        if s < half_y:
            w_ahead(s).start()
        if s < half_y - 1:
            w_behind(s).start()
        pending.extend(w_fresh(s))

    pending = []

    def w_exchange():
        for r in pending:
            for k in range(2):
                w_swap(r, k).start()
            w_twin(r).start()
        pending.clear()

    def w_far():
        b = w_all.at[:, c, :, cols_other]
        return send(b, b, sem_wf_s.at[ny], sem_wf_r.at[ny], me_e, sib)

    def w_end():
        for s in range(half_y + 1):
            for r in w_fresh(s):
                for k in range(2):
                    arrived(w_quarter(r, k, True), sem_wx_r.at[k, w_row(r)])
        w_far().start()

    def o_copy(j):
        to_x = (x + j) % nx
        return send(o_out.at[to_x], o_in.at[x], sem_o_s.at[j], sem_o_r.at[x], z * nx + to_x, me_t)

    score_scale = HD ** (-0.5) * math.log2(math.e)

    def kv_twin(way, m):
        zz = shard(way, m)
        return send(kv.at[zz, kv_mine], kv.at[zz, kv_mine], sem_kvf_s.at[zz], sem_kvf_r.at[zz], me_e, sib)

    def kv_ready(i):
        way, m = chain[i]
        zz = shard(way, m)
        arrived(kv.at[zz, kv_mine], sem_kv_r.at[zz])
        if kv_passes(way, m):
            kv_pass(way, m).start()
        kv_twin(way, m).start()

    def values_of(zz):
        rows = lax.broadcasted_iota(jnp.int32, (80, tq), 0)
        return jnp.where(rows < 16, 1.0, jnp.transpose(kv[zz].astype(F32))[48:128, :]).astype(BF16)

    def scores_of(zz, vt, xx):
        s_t = jnp.dot(kv[zz, :, 0:HD], q_all[xx], preferred_element_type=F32)
        p = jnp.exp2(s_t * score_scale).astype(BF16)
        return jnp.dot(vt, p, preferred_element_type=F32)

    def attend_own(part):
        vt = values_of(z)
        for j in range(nx) if part is None else ([0] if part == 0 else range(1, nx)):
            xx = (x + j) % nx
            if j:
                arrived(q_all.at[xx], sem_q_r.at[xx])
            o_acc[xx] = scores_of(z, vt, xx)

    def attend(i):
        last = i == len(chain) - 1
        zz = shard(*chain[i])
        arrived(kv.at[zz, kv_other], sem_kvf_r.at[zz])
        vt = values_of(zz)
        for j in range(1, nx + 1):
            xx = (x + j) % nx
            whole = o_acc[xx] + scores_of(zz, vt, xx)
            if last and j < nx:
                high = whole[0:8].astype(BF16)
                o_out[xx, 0:8] = high
                o_out[xx, 8:16] = (whole[8:16] - high.astype(F32)).astype(BF16)
                o_out[xx, 16:80] = whole[16:80].astype(BF16)
                o_copy(j).start()
            else:
                o_acc[xx] = whole

    own_at, other_at = par * (d // 2), (1 - par) * (d // 2)

    def swap(k, wave):
        at = al(own_at + k * feat + wave * fw, fw)
        b = slots.at[:, pl.ds(at, fw)]
        return send(b, b, sem_b_s.at[k, wave], sem_b_r.at[k, wave], me_e, leftward if k == 0 else right)

    def slots_ready(wave):
        for core in range(2):
            at = al(own_at + core * feat + wave * fw, fw)

            def one(j, _):
                arrived(
                    slots.at[pl.ds(al(j * SLOTS, SLOTS), SLOTS), pl.ds(at, fw)], sem_d_r.at[wave, j * 2 + core]
                )
                return 0

            lax.fori_loop(0, half_ep, one, 0)
            swap(core, wave).start()

    def half_products(start, first):
        for k in range(2):
            at = al(start + k * feat, feat)
            v = slots[:, pl.ds(at, feat)].astype(F32)
            sq = jnp.sum(v * v, axis=1, keepdims=True)
            scaled = (v * ffn_gain[:, pl.ds(at, feat)]).astype(BF16)
            for core in range(2):
                gp = jnp.dot(scaled, wg[core, pl.ds(at, feat), :], preferred_element_type=F32)
                up = jnp.dot(scaled, wu[core, pl.ds(at, feat), :], preferred_element_type=F32)
                if first and k == 0:
                    gate_acc[core], up_acc[core] = gp, up
                else:
                    gate_acc[core], up_acc[core] = gate_acc[core] + gp, up_acc[core] + up
            if first and k == 0:
                sq_acc[...] = jnp.broadcast_to(sq, sq_acc.shape)
            else:
                sq_acc[...] = sq_acc[...] + sq

    def ffn_first():
        for k in range(2):
            arrived(wg.at[1 - c], sem_ex_r.at[0]) if k == 0 else arrived(wu.at[1 - c], sem_ex_r.at[1])
        arrived(wd.at[pl.ds(al((1 - c) * ff, ff), ff)], sem_ex_r.at[2])
        half_products(own_at, True)

    def ffn_second():
        for k in range(2):
            for wave in range(2):
                arrived(slots.at[:, pl.ds(al(other_at + k * feat + wave * fw, fw), fw)], sem_b_r.at[k, wave])
        half_products(other_at, False)
        scale = lax.rsqrt(sq_acc[:, 0:1] * (1.0 / d) + EPSILON)
        for core in range(2):
            gate = scale * gate_acc[core]
            hidden[:, core * ff : (core + 1) * ff] = (
                gate / (1.0 + jnp.exp(-gate)) * (scale * up_acc[core])
            ).astype(BF16)
        ring_fill(0)

    yb = d // ny
    n_slots = half_ep * SLOTS
    hs = n_slots // 2

    def partial_of(dest):
        return jnp.dot(hidden[...], wd[:, pl.ds(al(dest * yb, yb), yb)], preferred_element_type=F32)

    cr = n_slots // CHUNKS

    def ring_has(way, s, k):
        return s > 0 or (k < CHUNKS // 2) == (way == 0)

    def ring_copy(way, s, k):
        rows = pl.ds(k * cr, cr)
        return send(
            ring_out.at[way, s, rows], ring_in.at[way, s, rows], sem_c_s.at[way, s, k], sem_c_r.at[way, s, k],
            me_e, right if way == 0 else leftward,
        )

    def ring_take(way, s, k, block):
        if not ring_has(way, s, k):
            return block
        rows = slice(k * cr, (k + 1) * cr)
        arrived(ring_in.at[way, s, pl.ds(k * cr, cr)], sem_c_r.at[way, s, k])
        return block + ring_in[way, s, rows].astype(F32)

    def ring_fill(s):
        for way in range(1 if s in (0, half_y) else 2):
            dest = (y + half_y - s) % ny if way == 0 else (y + ny - half_y + s) % ny
            ring_part[s % 2, way] = partial_of(dest)

    def ring_step(s):
        for j in range(CHUNKS):
            for way in range(2):
                k = (j + CHUNKS // 2) % CHUNKS if (s == 1 and way == 0) or (s != 1 and way == 1) else j
                if not ring_has(way, s, k):
                    continue
                rows = slice(k * cr, (k + 1) * cr)
                block = ring_part[s % 2, way if s else 0, rows]
                if s:
                    block = ring_take(way, s - 1, k, block)
                ring_out[way, s, rows] = block.astype(BF16)
                ring_copy(way, s, k).start()
        ring_fill(s + 1)

    def back_copy(j, core):
        src_e = c * half_ep + j
        return send(
            rows_out.at[core, pl.ds(al(j * SLOTS, SLOTS), SLOTS)],
            rows_in.at[pl.ds(al(me_e * SLOTS, SLOTS), SLOTS)],
            sem_r_s.at[j, core], sem_r_r.at[me_e], src_e, y * 2 + core,
        )

    def back_self(j, core):
        return pltpu.make_async_copy(
            rows_out.at[core, pl.ds(al(j * SLOTS, SLOTS), SLOTS)],
            rows_in.at[pl.ds(al(me_e * SLOTS, SLOTS), SLOTS)],
            sem_r_r.at[me_e],
        )

    def ring_end():
        s = half_y - 1

        def one(j, _):
            for core in range(2):
                here = (c * half_ep + j == me_e) & (c == core)

                @pl.when(here)
                def _():
                    back_self(j, core).start()

                @pl.when(jnp.logical_not(here))
                def _():
                    back_copy(j, core).start()

            return 0

        for k in range(CHUNKS):
            rows = slice(k * cr, (k + 1) * cr)
            block = ring_part[half_y % 2, 0, rows]
            for way in range(2):
                block = ring_take(way, s, k, block)
            block = block.astype(BF16)
            for core in range(2):
                rows_out[core, rows] = block[:, core * (yb // 2) : (core + 1) * (yb // 2)]
            per = half_ep // CHUNKS
            lax.fori_loop(k * per, (k + 1) * per, one, 0)

    def make_hot():
        fill = jnp.full((1, g.tok_pad - tok), -1, jnp.int32)
        rows = lax.broadcasted_iota(jnp.int32, (ep * SLOTS, g.tok_pad), 0)
        w0, w1 = scores[0:1, :], scores[1:2, :]
        whole = w0 + w1
        for k, (slot, w) in enumerate(((slot0, w0 / whole), (slot1, w1 / whole))):
            mask = (rows == jnp.concatenate([slot, fill], axis=1)).astype(F32)
            hot[k] = jnp.transpose(mask).astype(BF16)
            wide = jnp.concatenate([w, jnp.zeros((1, g.tok_pad - tok), F32)], axis=1)
            share[k] = jnp.transpose(jnp.broadcast_to(wide, (128, g.tok_pad)))

    def combine():
        def one(j, _):
            arrived(rows_in.at[pl.ds(al(j * SLOTS, SLOTS), SLOTS)], sem_r_r.at[j])
            return 0

        lax.fori_loop(0, ep, one, 0)
        p0 = jnp.dot(hot[0], rows_in[...], preferred_element_type=F32)
        p1 = jnp.dot(hot[1], rows_in[...], preferred_element_type=F32)
        expert_out[...] = (p0 * share[0] + p1 * share[1])[0:tok].astype(BF16)

    rows_t = tq // tp
    ht = rows_t // 2

    def a_copy(i):
        to_t = (me_t + i) % tp
        return send(
            att_out.at[pl.ds(al(to_t * ht, ht), ht)], att_in.at[pl.ds(al(me_t * ht, ht), ht)],
            sem_a_s.at[i], sem_a_r.at[me_t], me_e, to_t,
        )

    a_self = pltpu.make_async_copy(
        att_out.at[pl.ds(al(me_t * ht, ht), ht)], att_in.at[pl.ds(al(me_t * ht, ht), ht)], sem_a_r.at[me_t]
    )

    def attend_end():
        total = o_acc[x]
        numer, denom = total[16:80], total[0:8]
        for i in range(1, nx):
            xx = (x + i) % nx
            arrived(o_in.at[xx], sem_o_r.at[xx])
            numer = numer + o_in[xx, 16:80].astype(F32)
            denom = denom + o_in[xx, 0:8].astype(F32) + o_in[xx, 8:16].astype(F32)
        att_t = numer / denom[0:1]
        att = jnp.transpose(jnp.concatenate([att_t, att_t], axis=0))[:, 0:HD]
        for t in range(tp):
            at = t * rows_t
            att_out[t * ht : (t + 1) * ht, :] = jnp.concatenate(
                [att[at : at + ht], att[at + ht : at + rows_t]], axis=1
            ).astype(BF16)
        a_self.start()

        def one(i, _):
            a_copy(i).start()
            return 0

        lax.fori_loop(1, tp, one, 0)

    def project():
        def one(j, _):
            arrived(att_in.at[pl.ds(al(j * ht, ht), ht)], sem_a_r.at[j])
            return 0

        lax.fori_loop(0, tp, one, 0)

        for yy in range(ny):
            arrived(w_all.at[yy, 1 - c, :, cols_mine], sem_wf_r.at[yy])
        arrived(w_all.at[:, 1 - c, :, cols_other], sem_wf_r.at[ny])
        pieces = []
        for j in range(tp // 2):
            a = att_in[2 * j * ht : (2 * j + 1) * ht, :]
            b = att_in[(2 * j + 1) * ht : (2 * j + 2) * ht, :]
            top = jnp.concatenate([a[:, 0:HD], b[:, 0:HD]], axis=1)
            low_rows = jnp.concatenate([a[:, HD:], b[:, HD:]], axis=1)
            pieces.append(jnp.concatenate([top, low_rows], axis=0))
        lhs = jnp.concatenate(pieces, axis=1)
        mixed_out[...] = jnp.dot(lhs, w_all[...].reshape(tp * HD, d), preferred_element_type=F32).astype(BF16)

    w_step(0)
    plan = g.plan(half_y, len(chain))
    actions = dict(
        ffn1=ffn_first, ffn2=ffn_second, ring_end=ring_end,
        attend_end=attend_end, project=project, combine=combine, hot=make_hot, w_end=w_end, extra=extra_start, wx=w_exchange,
    )
    for name, arg in plan:
        with scope(name + str(arg)):
            if name == "kv":
                kv_ready(arg)
            elif name == "attend":
                attend(arg)
            elif name == "w":
                w_step(arg)
            elif name == "ring":
                ring_step(arg)
            elif name == "own":
                attend_own(arg)
            elif name == "slots":
                slots_ready(arg)
            else:
                actions[name]()

    for wave in range(2):

        def sent_dispatch(i, _):
            left(outbound.at[pl.ds(0, SLOTS), pl.ds(0, fw)], sem_d_s.at[wave, i])
            return 0

        lax.fori_loop(1, ep, sent_dispatch, 0)

        @pl.when(c != own_half)
        def _():
            left(outbound.at[pl.ds(0, SLOTS), pl.ds(0, fw)], sem_d_s.at[wave, 0])

    for i in range(1, nx):
        q_copy(i).wait_send()
        o_copy(i).wait_send()
    for way, m in [(1, 0), (-1, 0)] + chain:
        if kv_passes(way, m):
            kv_pass(way, m).wait_send()
        if m:
            kv_twin(way, m).wait_send()
    for copy in extra:
        copy.wait_send()
    for s in range(half_y):
        w_ahead(s).wait_send()
        if s < half_y - 1:
            w_behind(s).wait_send()
        for way in range(2):
            for k in range(CHUNKS):
                if ring_has(way, s, k):
                    ring_copy(way, s, k).wait_send()
    for k in range(2):
        for wave in range(2):
            swap(k, wave).wait_send()
    for s in range(half_y + 1):
        for r in w_fresh(s):
            w_twin(r).wait_send()
            for k in range(2):
                w_swap(r, k).wait_send()
    w_far().wait_send()

    def sent_back(j, _):
        for core in range(2):
            here = (c * half_ep + j == me_e) & (c == core)

            @pl.when(jnp.logical_not(here))
            def _():
                left(rows_out.at[core, pl.ds(0, SLOTS)], sem_r_s.at[j, core])

        return 0

    lax.fori_loop(0, half_ep, sent_back, 0)

    def sent_a(i, _):
        left(att_out.at[pl.ds(0, ht)], sem_a_s.at[i])
        return 0

    lax.fori_loop(1, tp, sent_a, 0)


PLAN = (
    "own0", "kv0", "kv1", "w1", "own1", "attend0", "extra", "w2", "slots0", "attend1", "slots1", "wx",
    "kv2", "kv3", "ffn1", "kv4", "kv5", "w3", "ffn2", "ring0", "attend2", "kv6", "attend3", "ring1", "attend4",
    "attend5", "ring2", "attend6", "w4", "wx", "hot", "ring3", "attend_end", "ring_end", "w_end",
    "project", "combine",
)


def default_plan(half_y, shards):
    plan = []
    for word in PLAN:
        name, arg = word.rstrip("0123456789"), word.lstrip("abcdefghijklmnopqrstuvwxyz_")
        if name == "ffn":
            name, arg = word, 0
        if name in ("kv", "attend") and int(arg) >= shards or name == "w" and int(arg) > half_y:
            continue
        if name == "ring" and int(arg) >= half_y:
            continue
        plan.append((name, int(arg or 0)))
    return plan


def local(g, queries, key_input, value_input, query_gain, key_gain, mix_out_weight, expert_input, ffn_gain,
          routes, route_scores, gate_weight, up_weight, down_weight):
    ep, tp = g.nz * g.nx, g.ny * 2
    tables = angle_tables(ep * g.tq // GRID_W)
    half_slots = ep // 2 * SLOTS
    vmem = pl.BlockSpec(memory_space=pltpu.VMEM)
    hbm = pl.BlockSpec(memory_space=pl.ANY)
    yb = g.d // g.ny
    half_y = g.ny // 2
    dma = pltpu.SemaphoreType.DMA
    return pl.pallas_call(
        functools.partial(kernel, g),
        out_shape=(
            jax.ShapeDtypeStruct((g.tq // tp, g.d), BF16),
            jax.ShapeDtypeStruct((g.tok, g.d // tp), BF16),
        ),
        in_specs=[hbm] * 17,
        out_specs=(vmem, vmem),
        scratch_shapes=[
            pltpu.VMEM((g.nz, g.tq, 2 * HD), BF16),
            pltpu.VMEM((HD, g.tq), BF16),
            pltpu.VMEM((g.nx, HD, g.tq), BF16),
            pltpu.VMEM((g.nx, 80, g.tq), F32),
            pltpu.VMEM((g.nx, 80, g.tq), BF16),
            pltpu.VMEM((g.nx, 80, g.tq), BF16),
            pltpu.VMEM((g.tq // 2, 2 * HD), BF16),
            pltpu.VMEM((g.tq // 2, 2 * HD), BF16),
            pltpu.VMEM((g.tq, 2 * HD), F32),
            pltpu.VMEM((g.ny, 2, HD, g.d), BF16),
            pltpu.VMEM((g.tok, g.d // 4), BF16),
            pltpu.VMEM((ep * SLOTS, g.d // 4), BF16),
            pltpu.VMEM((half_slots, g.d), BF16),
            pltpu.VMEM((2, g.d, g.ff), BF16),
            pltpu.VMEM((2, g.d, g.ff), BF16),
            pltpu.VMEM((2 * g.ff, g.d), BF16),
            pltpu.VMEM((2, half_slots, g.ff), F32),
            pltpu.VMEM((2, half_slots, g.ff), F32),
            pltpu.VMEM((half_slots, 128), F32),
            pltpu.VMEM((half_slots, 2 * g.ff), BF16),
            pltpu.VMEM((2, half_y, half_slots, yb), BF16),
            pltpu.VMEM((2, half_y, half_slots, yb), BF16),
            pltpu.VMEM((2, half_slots, yb // 2), BF16),
            pltpu.VMEM((ep * SLOTS, yb // 2), BF16),
            pltpu.VMEM((2, g.tok_pad, ep * SLOTS), BF16),
            pltpu.VMEM((2, g.tok_pad, 128), F32),
            pltpu.VMEM((2, 2, half_slots, yb), F32),
            pltpu.VMEM((HD, g.tq), BF16),
            pltpu.VMEM((g.tq, 2 * HD), BF16),
            pltpu.VMEM((g.tq, 2 * HD), BF16),
            pltpu.VMEM((1, HD), F32),
            pltpu.VMEM((1, HD), F32),
            pltpu.VMEM((g.tq // GRID_W, 2 * HD), F32),
            pltpu.VMEM((g.tq // GRID_W, 2 * HD), F32),
            pltpu.VMEM((GRID_W, 2 * HD), F32),
            pltpu.VMEM((GRID_W, 2 * HD), F32),
            pltpu.VMEM((2, g.tok), jnp.int32),
            pltpu.VMEM((2, g.tok), F32),
            pltpu.VMEM((1, g.d), F32),
            dma((17,)),
            dma((2, g.nz // 2)), dma((g.nz,)), dma((g.nz,)), dma((g.nz,)),
            dma((g.nx,)), dma((g.nx,)), dma((g.nx,)), dma((g.nx,)),
            dma((tp,)), dma((tp,)),
            dma((2, half_y)), dma((2, half_y)), dma((g.ny + 1,)), dma((g.ny + 1,)), dma((2, g.ny)), dma((2, g.ny)),
            dma((3,)), dma((3,)),
            dma((2, ep)), dma((2, ep)),
            dma((2, 2)), dma((2, 2)),
            dma((2, half_y, CHUNKS)), dma((2, half_y, CHUNKS)),
            dma((ep // 2, 2)), dma((ep,)),
        ],
        compiler_params=pltpu.CompilerParams(
            collective_id=0, has_side_effects=True, vmem_limit_bytes=62 * 1024 * 1024
        ),
    )(
        queries.T, key_input, value_input, key_gain.reshape(1, HD), query_gain.reshape(1, HD),
        *[jnp.asarray(t) for t in tables],
        expert_input, routes.T, route_scores.T, ffn_gain.reshape(1, g.d), mix_out_weight,
        gate_weight, up_weight, down_weight,
    )


SIZES = SimpleNamespace(nz=8, nx=4, ny=8, tq=512, tok=160, tok_pad=256, d=2048, ff=256, kv_heads=4, plan=default_plan)


def solution(mesh, g=SIZES):
    placed = (
        P("ep", "tp"),
        P("ep", None),
        P("ep", None),
        P(),
        P(),
        P("tp", None),
        P("ep", None),
        P(),
        P("ep", None),
        P("ep", None),
        P("ep", None, "tp"),
        P("ep", None, "tp"),
        P("ep", "tp", None),
    )
    return jax.shard_map(
        functools.partial(local, g),
        mesh=mesh,
        in_specs=placed,
        out_specs=(P(("ep", "tp"), None), P("ep", "tp")),
        check_vma=False,
    )
```

profile of v0, /device:TPU:1, one launch (start us, length us, event | category | flops | bytes accessed | tf_op | source)
XLA Modules:
  0.0 69.5 jit_solution(13370945984557670631)
XLA Ops:
  0.6 66.6 %shard_map.176 = (bf16[32,2048]{1,0:T(8,128)(2,1)}, bf16[160,128]{1,0:T(8,128)(2,1)}) custom-call(bf16[64,512]{1,0:T(8,128)(2,1)} %bitcast.6, bf16[512,256]{1,0:T(8,128)(2,1)} %keys_h.1, bf16[512,256]{1,0:T(8,128)(2,1)} %values_h.1, f32[1,64]{1,0:T(1,128)} %bitcast.10, f32[1,64]{1,0:T(1,128)} %bitcast.11, f32[256,128]{1,0:T(8,128)} %constant.8.clone.row_cos_h, ...), custom_call_target="tpu_custom_call" | custom-call | tf_op jit(solution)/shard_map/pallas_call | solution.py:802
  67.3 0.0 copy-start
  67.3 1.6 %copy.21 = bf16[32,2048]{1,0:T(8,128)(2,1)} copy(bf16[32,2048]{1,0:T(8,128)(2,1)} %get-tuple-element.4) | data formatting | bytes 262144
  68.9 0.0 copy-done
  68.9 0.6 copy.22
Async XLA Ops:
  67.3 1.6 %copy-start = (bf16[160,128]{1,0:T(8,128)(2,1)S(1)}, bf16[160,128]{1,0:T(8,128)(2,1)}, u32[]{:S(2)}) copy-start(bf16[160,128]{1,0:T(8,128)(2,1)} %get-tuple-element.5) | copy-start | bytes 122884
where the time goes:
time: 69.6 us; the launch traced here: 69.5 us
  Pallas kernels  66.6 us (96%)
  local copies, waits for them, and re-layouts  2.2 us (3%)
    pallas_call x1, Pallas kernels, local(): pl.pallas_call(functools.partial(kernel, g), out_shape=(jax.ShapeDtypeStr...  66.6 us
    unnamed x4, local copies, waits for them, and re-layouts  2.2 us

commit v1 on v0

--- a/solution.py
+++ b/solution.py
@@ -450,7 +450,7 @@
         zz = shard(*chain[i])
         arrived(kv.at[zz, kv_other], sem_kvf_r.at[zz])
         vt = values_of(zz)
-        for j in range(1, nx + 1):
+        for j in [nx // 2] + [j for j in range(1, nx + 1) if j != nx // 2]:
             xx = (x + j) % nx
             whole = o_acc[xx] + scores_of(zz, vt, xx)
             if last and j < nx:
@@ -769,8 +769,8 @@
 
 PLAN = (
     "own0", "kv0", "kv1", "w1", "own1", "attend0", "extra", "w2", "slots0", "attend1", "slots1", "wx",
-    "kv2", "kv3", "ffn1", "kv4", "kv5", "w3", "ffn2", "ring0", "attend2", "kv6", "attend3", "ring1", "attend4",
-    "attend5", "ring2", "attend6", "w4", "wx", "hot", "ring3", "attend_end", "ring_end", "w_end",
+    "kv2", "kv3", "ffn1", "attend2", "kv4", "kv5", "w3", "ffn2", "ring0", "attend3", "kv6", "ring1", "attend4",
+    "attend5", "ring2", "attend6", "hot", "w4", "wx", "ring3", "attend_end", "ring_end", "w_end",
     "project", "combine",
 )
 

time: 69.6 us -> 69.1 us (level)
  no operation moved by 1% of the time
where the time goes in v1:
time: 69.1 us; the launch traced here: 69 us
  Pallas kernels  66.1 us (96%)
  local copies, waits for them, and re-layouts  2.2 us (3%)
    pallas_call x1, Pallas kernels, local(): pl.pallas_call(functools.partial(kernel, g), out_shape=(jax.ShapeDtypeStr...  66.1 us
    unnamed x4, local copies, waits for them, and re-layouts  2.2 us

profile of v1, /device:TPU:1, one launch (start us, length us, event | category | flops | bytes accessed | tf_op | source)
XLA Modules:
  0.0 69.0 jit_solution(13126127766515623665)
XLA Ops:
  0.6 66.1 %shard_map.176 = (bf16[32,2048]{1,0:T(8,128)(2,1)}, bf16[160,128]{1,0:T(8,128)(2,1)}) custom-call(bf16[64,512]{1,0:T(8,128)(2,1)} %bitcast.6, bf16[512,256]{1,0:T(8,128)(2,1)} %keys_h.1, bf16[512,256]{1,0:T(8,128)(2,1)} %values_h.1, f32[1,64]{1,0:T(1,128)} %bitcast.10, f32[1,64]{1,0:T(1,128)} %bitcast.11, f32[256,128]{1,0:T(8,128)} %constant.8.clone.row_cos_h, ...), custom_call_target="tpu_custom_call" | custom-call | tf_op jit(solution)/shard_map/pallas_call | solution.py:802
  66.7 0.0 copy-start
  66.8 1.6 %copy.21 = bf16[32,2048]{1,0:T(8,128)(2,1)} copy(bf16[32,2048]{1,0:T(8,128)(2,1)} %get-tuple-element.4) | data formatting | bytes 262144
  68.3 0.0 copy-done
  68.3 0.6 copy.22
Async XLA Ops:
  66.7 1.6 %copy-start = (bf16[160,128]{1,0:T(8,128)(2,1)S(1)}, bf16[160,128]{1,0:T(8,128)(2,1)}, u32[]{:S(2)}) copy-start(bf16[160,128]{1,0:T(8,128)(2,1)} %get-tuple-element.5) | copy-start | bytes 122884
